TPU v7x, 512 devices: a whole 4x4x16 slice. The times are simulated.
512 devices in a mesh: gr: 2 (over z_hi), fs: 32 (over z_lo, y), tp: 8 (over x, core).
Axes of the slice: x: 4, y: 4, z: 16 (z_hi: 2, z_lo: 8; z = z_hi * 8 + z_lo), core: 2. Of those that a mesh axis runs over, the one named last changes fastest.
Arguments:
- tokens: bfloat16 [24576, 2048], P(('gr', 'fs')), may hold values from -6 to 6
- route_ids: int32 [24576, 2], P(('gr', 'fs')), may hold values from 0 to 31, as said below
- route_weights: float32 [24576, 2], P(('gr', 'fs')), may hold values from 0.1 to 1
- norm_gain: float32 [2048], P(('gr', 'fs')), may hold values from 0.1 to 1.9
- gate_weight: float32 [32, 2048, 1024], P(None, ('gr', 'fs'), 'tp'), may hold values from -0.125 to 0.125
- up_weight: float32 [32, 2048, 1024], P(None, ('gr', 'fs'), 'tp'), may hold values from -0.125 to 0.125
- down_weight: float32 [32, 1024, 2048], P(None, ('gr', 'fs'), 'tp'), may hold values from -0.1875 to 0.1875
Outputs:
- gate_new: bfloat16 [32, 2048, 1024], P('fs', None, 'tp')
- up_new: bfloat16 [32, 2048, 1024], P('fs', None, 'tp')
- down_new: bfloat16 [32, 1024, 2048], P('fs', 'tp')
- mixed: bfloat16 [24576, 2048], P(('gr', 'fs'), 'tp')
Inputs may be any that keep to these rules, and one draw needn't show every extreme that they name: `route_ids`: each row names two different experts of one group (expert e belongs to group e // 8); in each device's block of 384 rows every expert is named by exactly 24 rows.
All inputs are finite; a program needn't handle non-finite values.
Results may differ from a plain program's by a relative error of at most 0.015.
Values may be sent and summed in bfloat16 or wider, within the bound.
A program may use at most 64 MiB of HBM per device.

v0:
```python
import jax
import jax.numpy as jnp
from jax import lax
from jax.sharding import Mesh
from jax.sharding import PartitionSpec as P

TP = ("tp_0", "tp_1")


def side_by_side(arrays, axis, split_dim, concat_dim, along):
    ends, at = ([], 0)
    for a in arrays[:-1]:
        at += a.shape[along]
        ends.append(at)
    both = jnp.concatenate(arrays, axis=along)
    return tuple(
        jnp.split(
            lax.all_to_all(both, axis, split_axis=split_dim, concat_axis=concat_dim, tiled=True),
            ends,
            axis=along,
        )
    )


def in_one_piece(arrays, axis, dim, along):
    ends, at = ([], 0)
    for a in arrays[:-1]:
        at += a.shape[along]
        ends.append(at)
    both = jnp.concatenate(arrays, axis=along)
    return tuple(jnp.split(lax.all_gather(both, axis, axis=dim, tiled=True), ends, axis=along))


def split_up(array, dim, devices):
    before, after = (array.shape[:dim], array.shape[dim + 1 :])
    return jnp.moveaxis(array.reshape(*before, devices, -1, *after), dim, 0)


def laid_out(pieces, dim):
    pieces = jnp.moveaxis(pieces, 0, dim)
    lengths = pieces.shape
    return pieces.reshape(*lengths[:dim], lengths[dim] * lengths[dim + 1], *lengths[dim + 2 :])


def exchange_in_order(pieces, axes, turns):
    inside = pieces.shape[1:]
    whole = pieces.reshape(*(lax.axis_size(a) for a in axes), *inside)
    for k in turns:
        whole = lax.all_to_all(whole, axes[k], k, k, tiled=True)
    return whole.reshape(-1, *inside)


def exchange_by_axis(array, axes, turns, split_dim, concat_dim):
    pieces = split_up(array, split_dim, lax.axis_size(axes))
    return laid_out(exchange_in_order(pieces, axes, turns), concat_dim)


def local(tokens, route_ids, route_weights, norm_gain, gate_weight, up_weight, down_weight):
    gate_folded = (gate_weight * norm_gain[None, :, None]).astype(jnp.bfloat16)
    up_folded = (up_weight * norm_gain[None, :, None]).astype(jnp.bfloat16)
    down_rounded = down_weight.astype(jnp.bfloat16)
    moved = (
        *side_by_side((gate_folded, up_folded), "fs", 0, 1, 2),
        lax.all_to_all(down_rounded, "fs", split_axis=0, concat_axis=1, tiled=True),
    )
    gate_new, up_new, down_whole = (
        *in_one_piece((moved[0], moved[1]), "gr", 1, 0),
        lax.all_gather(moved[2], "gr", axis=1, tiled=True),
    )
    down_new = exchange_by_axis(down_whole, TP, (1, 0), 1, 2)
    tok = tokens.shape[0]
    width = tokens.shape[1]
    experts = gate_weight.shape[0]
    cap = 2 * tok // experts
    flat_ids = route_ids.reshape(-1)
    onehot = (flat_ids[:, None] == jnp.arange(experts, dtype=jnp.int32)[None, :]).astype(jnp.int32)
    slot = jnp.sum(jnp.cumsum(onehot, axis=0) * onehot, axis=1) - 1
    position = flat_ids * cap + slot
    source = (
        jnp.zeros((experts * cap,), jnp.int32)
        .at[position]
        .set(jnp.arange(2 * tok, dtype=jnp.int32) // 2)
    )
    widened = tokens.astype(jnp.float32)
    normed = (
        widened * lax.rsqrt(jnp.mean(widened * widened, axis=-1, keepdims=True) + 1e-06)
    ).astype(jnp.bfloat16)
    outgoing = normed[source].reshape(experts, cap, width)
    received = lax.all_to_all(outgoing, "fs", split_axis=0, concat_axis=0, tiled=True)
    senders, count, _ = received.shape
    rows = received.reshape(senders * count, width)
    first = jnp.dot(rows, gate_new[0], preferred_element_type=jnp.float32)
    second = jnp.dot(rows, up_new[0], preferred_element_type=jnp.float32)
    hidden = (jax.nn.silu(first) * second).astype(jnp.bfloat16)
    hidden_width = hidden.shape[1]
    down_local = down_whole[0]
    out_columns = down_local.shape[1]
    row_count = hidden.shape[0]
    piece = lax.all_gather(hidden, TP, axis=1, tiled=True)
    piece_width = piece.shape[1]
    blocks = piece_width // hidden_width
    partials = jnp.einsum(
        "mbf,bfd->bmd",
        piece.reshape(row_count, blocks, hidden_width),
        down_local.reshape(blocks, hidden_width, out_columns),
        preferred_element_type=jnp.float32,
    ).astype(jnp.bfloat16)
    total = jnp.sum(partials.astype(jnp.float32), axis=0)
    summed = total.reshape(senders, count, out_columns)
    returned = lax.all_to_all(
        summed.astype(jnp.bfloat16), "fs", split_axis=0, concat_axis=0, tiled=True
    )
    columns = returned.shape[2]
    route_out = returned.reshape(experts * cap, columns)[position].reshape(tok, 2, columns)
    mixed = jnp.sum(route_weights[:, :, None] * route_out.astype(jnp.float32), axis=1).astype(
        jnp.bfloat16
    )
    return (gate_new, up_new, down_new, mixed)


def solution(mesh):
    torus = Mesh(
        mesh.devices.reshape(mesh.shape["gr"], mesh.shape["fs"], 4, 2), ("gr", "fs", "tp_0", "tp_1")
    )
    placed = (
        P(("gr", "fs"), None),
        P(("gr", "fs"), None),
        P(("gr", "fs"), None),
        P(("gr", "fs")),
        P(None, ("gr", "fs"), TP),
        P(None, ("gr", "fs"), TP),
        P(None, ("gr", "fs"), TP),
    )
    return jax.shard_map(
        local,
        mesh=torus,
        in_specs=placed,
        out_specs=(P("fs", None, TP), P("fs", None, TP), P("fs", TP, None), P(("gr", "fs"), TP)),
        check_vma=False,
    )
```

profile of v0, /device:TPU:2, one launch (start us, length us, event | category | flops | bytes accessed | tf_op | source)
XLA Modules:
  0.0 370.6 jit_solution(3223288350482646378)
XLA Ops:
  7.2 1.5 multiply_convert_fusion.1
  8.7 0.9 pad_maximum_fusion
  9.6 15.7 %all-to-all-start = ((bf16[32,32,256]{2,1,0:T(8,128)(2,1)}), bf16[32,32,256]{2,1,0:T(8,128)(2,1)}, u32[]{:S(2)}, u32[]{:S(2)}) async-start(bf16[32,32,256]{2,1,0:T(8,128)(2,1)} %pad_maximum_fusion), calls=%async_computation | async-start | bytes 1048576 | tf_op jit(solution)/shard_map/all_to_all | solution.py:18
  25.7 1.7 reduce-window.6
  27.4 0.3 slice_reduce_fusion
  28.2 3.4 scatter_custom_fusion
  31.6 0.4 fusion
  32.0 0.3 fusion.1
  32.4 4.3 %gather_fusion = bf16[768,2048]{1,0:T(8,128)(2,1)} fusion(bf16[384,2048]{1,0:T(8,128)(2,1)S(1)} %fusion.1, s32[1024]{0:T(1024)S(1)} %pad_clamp_fusion.1), kind=kCustom, calls=%fused_computation | custom fusion | bytes 6294528 | tf_op jit(solution)/shard_map/gather | solution.py:88
  36.6 18.2 %all-to-all-done = bf16[32,32,256]{2,1,0:T(8,128)(2,1)} async-done(((bf16[32,32,256]{2,1,0:T(8,128)(2,1)}), bf16[32,32,256]{2,1,0:T(8,128)(2,1)}, u32[]{:S(2)}, u32[]{:S(2)}) %all-to-all-start) | async-done | bytes 524320 | tf_op jit(solution)/shard_map/all_to_all | solution.py:18
  54.8 6.1 %all-to-all-start.4 = ((bf16[32,24,2048]{2,1,0:T(8,128)(2,1)}), bf16[32,24,2048]{2,1,0:T(8,128)(2,1)S(1)}, u32[]{:S(2)}, u32[]{:S(2)}) async-start(bf16[32,24,2048]{2,1,0:T(8,128)(2,1)} %bitcast.48), calls=%async_computation.4 | async-start | bytes 6291456 | tf_op jit(solution)/shard_map/all_to_all | solution.py:89
  61.0 1.1 fusion.18
  62.1 0.8 pad_maximum_fusion.1
  63.0 66.8 %all-gather.3.cloned.1.call-done = bf16[2,2048,128]{2,1,0:T(8,128)(2,1)} async-done(((bf16[2,1024,128]{2,1,0:T(8,128)(2,1)}), bf16[2,2048,128]{2,1,0:T(8,128)(2,1)}) %all-gather.3.cloned.1.call-update) | async-done | bytes 1048592 | tf_op jit(solution)/shard_map/all_gather | solution.py:31
  129.8 2.2 fusion.17
  132.0 114.4 %all-to-all-done.4 = bf16[32,24,2048]{2,1,0:T(8,128)(2,1)S(1)} async-done(((bf16[32,24,2048]{2,1,0:T(8,128)(2,1)}), bf16[32,24,2048]{2,1,0:T(8,128)(2,1)S(1)}, u32[]{:S(2)}, u32[]{:S(2)}) %all-to-all-start.4) | async-done | bytes 3145760 | tf_op jit(solution)/shard_map/all_to_all | solution.py:89
  246.4 2.1 fusion.6
  248.5 1.7 fusion.4
  250.2 1.1 convert_element_type.42
  251.3 26.3 %all_to_all.44 = bf16[32,16,256]{2,1,0:T(8,128)(2,1)S(1)} all-to-all(bf16[32,16,256]{2,1,0:T(8,128)(2,1)S(1)} %convert_element_type.42), channel_id=1, replica_groups=mesh['gr'=2,'fs'=32,'tp_0'=4,'tp_1'=2] {'fs'}, dimensions={0} | all-to-all | bytes 524288 | tf_op jit(solution)/shard_map/all_to_all | solution.py:64
  277.6 29.7 %all_gather.10 = bf16[1,1024,256]{2,1,0:T(8,128)(2,1)S(1)} all-gather(bf16[1,512,256]{2,1,0:T(8,128)(2,1)S(1)} %bitcast.52), channel_id=1, replica_groups=mesh['gr'=2,'fs'=32,'tp_0'=4,'tp_1'=2] {'gr'}, dimensions={1}, use_global_device_ids=true | all-gather | bytes 786432 | tf_op jit(solution)/shard_map/all_gather | solution.py:68
  307.3 4.2 %all_to_all.45 = bf16[4,2,1,128,256]{4,3,0,2,1:T(8,128)(2,1)S(1)} all-to-all(bf16[4,2,1,128,256]{4,3,0,2,1:T(8,128)(2,1)S(1)} %copy.29), channel_id=1, replica_groups=mesh['gr'=2,'fs'=32,'tp_0'=4,'tp_1'=2] {'tp_1'}, dimensions={1} | all-to-all | bytes 1048576 | tf_op jit(solution)/shard_map/all_to_all | solution.py:49
  311.5 0.8 copy.30
  312.3 5.0 %all-to-all-start.3 = ((bf16[4,2,1,128,256]{4,3,1,2,0:T(8,128)(2,1)}), bf16[4,2,1,128,256]{4,3,1,2,0:T(8,128)(2,1)S(1)}, u32[]{:S(2)}, u32[]{:S(2)}) async-start(bf16[4,2,1,128,256]{4,3,1,2,0:T(8,128)(2,1)} %copy.30), calls=%async_computation.3 | async-start | bytes 1048576 | tf_op jit(solution)/shard_map/all_to_all | solution.py:49
  317.3 3.2 convert_reduce_fusion
  320.5 5.1 %all-to-all-done.3 = bf16[4,2,1,128,256]{4,3,1,2,0:T(8,128)(2,1)S(1)} async-done(((bf16[4,2,1,128,256]{4,3,1,2,0:T(8,128)(2,1)}), bf16[4,2,1,128,256]{4,3,1,2,0:T(8,128)(2,1)S(1)}, u32[]{:S(2)}, u32[]{:S(2)}) %all-to-all-start.3) | async-done | bytes 524320 | tf_op jit(solution)/shard_map/all_to_all | solution.py:49
  325.6 10.0 %all-to-all-start.5 = ((bf16[32,24,256]{2,1,0:T(8,128)(2,1)}), bf16[32,24,256]{2,1,0:T(8,128)(2,1)S(1)}, u32[]{:S(2)}, u32[]{:S(2)}) async-start(bf16[32,24,256]{2,1,0:T(8,128)(2,1)} %bitcast.11), calls=%async_computation.5 | async-start | bytes 786432 | tf_op jit(solution)/shard_map/all_to_all | solution.py:110
  335.7 0.8 copy.39
  336.6 22.4 %all-to-all-done.5 = bf16[32,24,256]{2,1,0:T(8,128)(2,1)S(1)} async-done(((bf16[32,24,256]{2,1,0:T(8,128)(2,1)}), bf16[32,24,256]{2,1,0:T(8,128)(2,1)S(1)}, u32[]{:S(2)}, u32[]{:S(2)}) %all-to-all-start.5) | async-done | bytes 393248 | tf_op jit(solution)/shard_map/all_to_all | solution.py:110
  359.0 2.6 gather_fusion.1
  361.6 0.4 reshape.105
  362.0 1.7 multiply_reduce_fusion
  (31 shorter events, 1.2 us)
Async XLA Ops:
  7.2 18.1 %copy-start.2 = (s32[384,2]{0,1:T(2,128)S(1)}, s32[384,2]{0,1:T(2,128)}, u32[]{:S(2)}) copy-start(s32[384,2]{0,1:T(2,128)} %param.8) | copy-start | bytes 9220
  7.2 24.4 %copy-start = (bf16[384,2048]{1,0:T(8,128)(2,1)S(1)}, bf16[384,2048]{1,0:T(8,128)(2,1)}, u32[]{:S(2)}) copy-start(bf16[384,2048]{1,0:T(8,128)(2,1)} %param.7) | copy-start | bytes 4718596
  9.6 45.3 %all-to-all-start = ((bf16[32,32,256]{2,1,0:T(8,128)(2,1)}), bf16[32,32,256]{2,1,0:T(8,128)(2,1)}, u32[]{:S(2)}, u32[]{:S(2)}) async-start(bf16[32,32,256]{2,1,0:T(8,128)(2,1)} %pad_maximum_fusion), calls=%async_computation | async-start | bytes 1048576 | tf_op jit(solution)/shard_map/all_to_all | solution.py:18
  54.8 191.6 %all-to-all-start.4 = ((bf16[32,24,2048]{2,1,0:T(8,128)(2,1)}), bf16[32,24,2048]{2,1,0:T(8,128)(2,1)S(1)}, u32[]{:S(2)}, u32[]{:S(2)}) async-start(bf16[32,24,2048]{2,1,0:T(8,128)(2,1)} %bitcast.48), calls=%async_computation.4 | async-start | bytes 6291456 | tf_op jit(solution)/shard_map/all_to_all | solution.py:89
  60.9 68.8 %all-gather.3.cloned.1.call-start = ((), (), s32[]{:S(2)}) async-start(), calls=%async_computation.6 | async-start | bytes 1572864 | tf_op jit(solution)/shard_map/all_gather | solution.py:31
  62.9 254.4 %all-gather.5.cloned.1.call-start = ((), (), s32[]{:S(2)}) async-start(), calls=%async_computation.7 | async-start | bytes 1769472 | tf_op jit(solution)/shard_map/all_gather | solution.py:99
  246.4 2.1 copy-start.1
  312.3 23.3 %copy-start.3 = (f32[384,2]{0,1:T(2,128)S(1)}, f32[384,2]{0,1:T(2,128)}, u32[]{:S(2)}) copy-start(f32[384,2]{0,1:T(2,128)} %param.9) | copy-start | bytes 9220
  312.3 13.3 %all-to-all-start.3 = ((bf16[4,2,1,128,256]{4,3,1,2,0:T(8,128)(2,1)}), bf16[4,2,1,128,256]{4,3,1,2,0:T(8,128)(2,1)S(1)}, u32[]{:S(2)}, u32[]{:S(2)}) async-start(bf16[4,2,1,128,256]{4,3,1,2,0:T(8,128)(2,1)} %copy.30), calls=%async_computation.3 | async-start | bytes 1048576 | tf_op jit(solution)/shard_map/all_to_all | solution.py:49
  325.6 33.4 %all-to-all-start.5 = ((bf16[32,24,256]{2,1,0:T(8,128)(2,1)}), bf16[32,24,256]{2,1,0:T(8,128)(2,1)S(1)}, u32[]{:S(2)}, u32[]{:S(2)}) async-start(bf16[32,24,256]{2,1,0:T(8,128)(2,1)} %bitcast.11), calls=%async_computation.5 | async-start | bytes 786432 | tf_op jit(solution)/shard_map/all_to_all | solution.py:110
Sparse Core Ops, SparseCore 0:
  64.4 65.2 all-gather.2
  250.3 28.7 all-gather.4
where the time goes:
time: 371 us
  waiting for transfers between devices  227 us (61%)
  blocking collectives  60.1 us (16%)
  starting transfers between devices  36.8 us (10%)
  local copies, waits for them, and re-layouts  16.8 us (5%)
  between operations  14.3 us (4%)
  other arithmetic  8.64 us (2%)
  matrix products  6.94 us (2%)
    all_to_all x1, waiting for transfers between devices, local(): lax.all_to_all(outgoing, 'fs', split_axis=0, concat_axis=0, tiled=True)  114 us
    all_gather x1, waiting for transfers between devices, in_one_piece(): lax.all_gather(both, axis, axis=dim, tiled=True)  66.8 us
    all_gather x1, blocking collectives, local(): lax.all_gather(moved[2], 'gr', axis=1, tiled=True)  29.7 us
    all_to_all x1, blocking collectives, local(): lax.all_to_all(down_rounded, 'fs', split_axis=0, concat_axis=1, tiled=True)  26.3 us
    all_to_all x1, waiting for transfers between devices, local(): lax.all_to_all(summed.astype(jnp.bfloat16), 'fs', split_axis=0, concat_ax...  22.4 us
    all_to_all x1, waiting for transfers between devices, side_by_side(): lax.all_to_all(both, axis, split_axis=split_dim, concat_axis=concat_dim,...  18.2 us
    all_to_all x1, starting transfers between devices, side_by_side(): lax.all_to_all(both, axis, split_axis=split_dim, concat_axis=concat_dim,...  15.7 us
    all_to_all x1, starting transfers between devices, local(): lax.all_to_all(summed.astype(jnp.bfloat16), 'fs', split_axis=0, concat_ax...  9.96 us
  transfers between devices with their start and end apart: 6, of which 5 were waited for; matrix products, arithmetic and copies ran while one was open for 6% of the time, Pallas kernels for 0%

commit v1 on v0

--- a/solution.py
+++ b/solution.py
@@ -61,7 +61,12 @@
     down_rounded = down_weight.astype(jnp.bfloat16)
     moved = (
         *side_by_side((gate_folded, up_folded), "fs", 0, 1, 2),
-        lax.all_to_all(down_rounded, "fs", split_axis=0, concat_axis=1, tiled=True),
+        jnp.concatenate(
+            lax.all_to_all(
+                jnp.stack(jnp.split(down_rounded, lax.axis_size("fs"), axis=0)), "fs", 0, 0
+            ),
+            axis=1,
+        ),
     )
     gate_new, up_new, down_whole = (
         *in_one_piece((moved[0], moved[1]), "gr", 1, 0),

time: 371 us -> 375 us (1.011)
  local copies, waits for them, and re-layouts: 16.8 us -> 24.7 us
  waiting for transfers between devices: 227 us -> 222 us
    unnamed x10 -> x43, local copies, waits for them, and re-layouts: 0.29 us -> 7.57 us
    all_gather x1, waiting for transfers between devices: 66.8 us -> 62.3 us  [in_one_piece(): lax.all_gather(both, axis, axis=dim, tiled=True)]
  transfers between devices with their start and end apart: 6 -> 6, of which waited for: 5 -> 5; matrix products, arithmetic and copies ran while one was open for 6% -> 8% of each run, Pallas kernels for 0% -> 0%
where the time goes in v1:
time: 375 us; the launch traced here: 374 us
  waiting for transfers between devices  222 us (59%)
  blocking collectives  60.3 us (16%)
  starting transfers between devices  36.8 us (10%)
  local copies, waits for them, and re-layouts  24.7 us (7%)
  between operations  14.4 us (4%)
  other arithmetic  8.64 us (2%)
  matrix products  6.94 us (2%)
    all_to_all x1, waiting for transfers between devices, local(): lax.all_to_all(outgoing, 'fs', split_axis=0, concat_axis=0, tiled=True)  114 us
    all_gather x1, waiting for transfers between devices, in_one_piece(): lax.all_gather(both, axis, axis=dim, tiled=True)  62.3 us
    all_gather x1, blocking collectives, local(): lax.all_gather(moved[2], 'gr', axis=1, tiled=True)  29.7 us
    all_to_all x1, blocking collectives, local(): lax.all_to_all(jnp.stack(jnp.split(down_rounded, lax.axis_size('fs'), axi...  26.5 us
    all_to_all x1, waiting for transfers between devices, local(): lax.all_to_all(summed.astype(jnp.bfloat16), 'fs', split_axis=0, concat_ax...  22.4 us
    all_to_all x1, waiting for transfers between devices, side_by_side(): lax.all_to_all(both, axis, split_axis=split_dim, concat_axis=concat_dim,...  18.2 us
    all_to_all x1, starting transfers between devices, side_by_side(): lax.all_to_all(both, axis, split_axis=split_dim, concat_axis=concat_dim,...  15.7 us
    all_to_all x1, starting transfers between devices, local(): lax.all_to_all(summed.astype(jnp.bfloat16), 'fs', split_axis=0, concat_ax...  9.97 us
  transfers between devices with their start and end apart: 6, of which 5 were waited for; matrix products, arithmetic and copies ran while one was open for 8% of the time, Pallas kernels for 0%

profile of v1, /device:TPU:2, one launch (start us, length us, event | category | flops | bytes accessed | tf_op | source)
XLA Modules:
  0.0 373.9 jit_solution(5655376793444644242)
XLA Ops:
  7.2 1.5 multiply_convert_fusion.1
  8.7 0.9 pad_maximum_fusion
  9.6 15.7 %all-to-all-start = ((bf16[32,32,256]{2,1,0:T(8,128)(2,1)}), bf16[32,32,256]{2,1,0:T(8,128)(2,1)}, u32[]{:S(2)}, u32[]{:S(2)}) async-start(bf16[32,32,256]{2,1,0:T(8,128)(2,1)} %pad_maximum_fusion), calls=%async_computation | async-start | bytes 1048576 | tf_op jit(solution)/shard_map/all_to_all | solution.py:18
  25.7 1.7 reduce-window.6
  28.2 3.4 scatter_custom_fusion
  32.4 4.3 %gather_fusion = bf16[768,2048]{1,0:T(8,128)(2,1)} fusion(bf16[384,2048]{1,0:T(8,128)(2,1)S(1)} %fusion.1, s32[1024]{0:T(1024)S(1)} %pad_clamp_fusion.1), kind=kCustom, calls=%fused_computation | custom fusion | bytes 6294528 | tf_op jit(solution)/shard_map/gather | solution.py:93
  36.6 18.2 %all-to-all-done = bf16[32,32,256]{2,1,0:T(8,128)(2,1)} async-done(((bf16[32,32,256]{2,1,0:T(8,128)(2,1)}), bf16[32,32,256]{2,1,0:T(8,128)(2,1)}, u32[]{:S(2)}, u32[]{:S(2)}) %all-to-all-start) | async-done | bytes 524320 | tf_op jit(solution)/shard_map/all_to_all | solution.py:18
  54.8 6.1 %all-to-all-start.4 = ((bf16[32,24,2048]{2,1,0:T(8,128)(2,1)}), bf16[32,24,2048]{2,1,0:T(8,128)(2,1)S(1)}, u32[]{:S(2)}, u32[]{:S(2)}) async-start(bf16[32,24,2048]{2,1,0:T(8,128)(2,1)} %bitcast.176), calls=%async_computation.4 | async-start | bytes 6291456 | tf_op jit(solution)/shard_map/all_to_all | solution.py:94
  61.0 1.1 convert_element_type.42
  62.3 0.7 copy-done.2
  63.0 1.1 fusion.18
  64.0 0.8 pad_maximum_fusion.1
  67.9 62.3 %all-gather.3.cloned.1.call-done = bf16[2,2048,128]{2,1,0:T(8,128)(2,1)} async-done(((bf16[2,1024,128]{2,1,0:T(8,128)(2,1)}), bf16[2,2048,128]{2,1,0:T(8,128)(2,1)}) %all-gather.3.cloned.1.call-update) | async-done | bytes 1048592 | tf_op jit(solution)/shard_map/all_gather | solution.py:31
  130.2 2.2 fusion.17
  132.4 114.0 %all-to-all-done.4 = bf16[32,24,2048]{2,1,0:T(8,128)(2,1)S(1)} async-done(((bf16[32,24,2048]{2,1,0:T(8,128)(2,1)}), bf16[32,24,2048]{2,1,0:T(8,128)(2,1)S(1)}, u32[]{:S(2)}, u32[]{:S(2)}) %all-to-all-start.4) | async-done | bytes 3145760 | tf_op jit(solution)/shard_map/all_to_all | solution.py:94
  246.4 2.1 fusion.6
  248.5 1.7 fusion.4
  250.2 0.6 constant_dynamic-update-slice_fusion.6
  250.8 0.6 constant_dynamic-update-slice_fusion.5
  253.8 0.6 constant_dynamic-update-slice_fusion
  254.4 26.5 %all_to_all.37 = bf16[32,1,16,256]{3,2,1,0:T(8,128)(2,1)S(1)} all-to-all(bf16[32,1,16,256]{3,2,1,0:T(8,128)(2,1)} %constant_dynamic-update-slice_fusion), channel_id=1, replica_groups=mesh['gr'=2,'fs'=32,'tp_0'=4,'tp_1'=2] {'fs'}, dimensions={0} | all-to-all | bytes 524288 | tf_op jit(solution)/shard_map/all_to_all | solution.py:65
  280.9 29.7 %all_gather.10 = bf16[1,1024,256]{2,1,0:T(8,128)(2,1)S(1)} all-gather(bf16[1,512,256]{2,1,0:T(8,128)(2,1)S(1)} %bitcast.180), channel_id=1, replica_groups=mesh['gr'=2,'fs'=32,'tp_0'=4,'tp_1'=2] {'gr'}, dimensions={1}, use_global_device_ids=true | all-gather | bytes 786432 | tf_op jit(solution)/shard_map/all_gather | solution.py:73
  310.6 4.2 %all_to_all.38 = bf16[4,2,1,128,256]{4,3,0,2,1:T(8,128)(2,1)S(1)} all-to-all(bf16[4,2,1,128,256]{4,3,0,2,1:T(8,128)(2,1)S(1)} %copy.29), channel_id=1, replica_groups=mesh['gr'=2,'fs'=32,'tp_0'=4,'tp_1'=2] {'tp_1'}, dimensions={1} | all-to-all | bytes 1048576 | tf_op jit(solution)/shard_map/all_to_all | solution.py:49
  314.8 0.8 copy.30
  315.6 5.0 %all-to-all-start.3 = ((bf16[4,2,1,128,256]{4,3,1,2,0:T(8,128)(2,1)}), bf16[4,2,1,128,256]{4,3,1,2,0:T(8,128)(2,1)S(1)}, u32[]{:S(2)}, u32[]{:S(2)}) async-start(bf16[4,2,1,128,256]{4,3,1,2,0:T(8,128)(2,1)} %copy.30), calls=%async_computation.3 | async-start | bytes 1048576 | tf_op jit(solution)/shard_map/all_to_all | solution.py:49
  320.6 3.2 convert_reduce_fusion
  323.8 5.1 %all-to-all-done.3 = bf16[4,2,1,128,256]{4,3,1,2,0:T(8,128)(2,1)S(1)} async-done(((bf16[4,2,1,128,256]{4,3,1,2,0:T(8,128)(2,1)}), bf16[4,2,1,128,256]{4,3,1,2,0:T(8,128)(2,1)S(1)}, u32[]{:S(2)}, u32[]{:S(2)}) %all-to-all-start.3) | async-done | bytes 524320 | tf_op jit(solution)/shard_map/all_to_all | solution.py:49
  328.9 10.0 %all-to-all-start.5 = ((bf16[32,24,256]{2,1,0:T(8,128)(2,1)}), bf16[32,24,256]{2,1,0:T(8,128)(2,1)S(1)}, u32[]{:S(2)}, u32[]{:S(2)}) async-start(bf16[32,24,256]{2,1,0:T(8,128)(2,1)} %bitcast.43), calls=%async_computation.5 | async-start | bytes 786432 | tf_op jit(solution)/shard_map/all_to_all | solution.py:115
  339.0 0.8 copy.39
  339.9 22.4 %all-to-all-done.5 = bf16[32,24,256]{2,1,0:T(8,128)(2,1)S(1)} async-done(((bf16[32,24,256]{2,1,0:T(8,128)(2,1)}), bf16[32,24,256]{2,1,0:T(8,128)(2,1)S(1)}, u32[]{:S(2)}, u32[]{:S(2)}) %all-to-all-start.5) | async-done | bytes 393248 | tf_op jit(solution)/shard_map/all_to_all | solution.py:115
  362.3 2.6 gather_fusion.1
  365.3 1.7 multiply_reduce_fusion
  (65 shorter events, 8.0 us)
Async XLA Ops:
  7.2 18.1 %copy-start.3 = (s32[384,2]{0,1:T(2,128)S(1)}, s32[384,2]{0,1:T(2,128)}, u32[]{:S(2)}) copy-start(s32[384,2]{0,1:T(2,128)} %param.8) | copy-start | bytes 9220
  7.2 24.4 %copy-start = (bf16[384,2048]{1,0:T(8,128)(2,1)S(1)}, bf16[384,2048]{1,0:T(8,128)(2,1)}, u32[]{:S(2)}) copy-start(bf16[384,2048]{1,0:T(8,128)(2,1)} %param.7) | copy-start | bytes 4718596
  9.6 45.3 %all-to-all-start = ((bf16[32,32,256]{2,1,0:T(8,128)(2,1)}), bf16[32,32,256]{2,1,0:T(8,128)(2,1)}, u32[]{:S(2)}, u32[]{:S(2)}) async-start(bf16[32,32,256]{2,1,0:T(8,128)(2,1)} %pad_maximum_fusion), calls=%async_computation | async-start | bytes 1048576 | tf_op jit(solution)/shard_map/all_to_all | solution.py:18
  54.8 191.6 %all-to-all-start.4 = ((bf16[32,24,2048]{2,1,0:T(8,128)(2,1)}), bf16[32,24,2048]{2,1,0:T(8,128)(2,1)S(1)}, u32[]{:S(2)}, u32[]{:S(2)}) async-start(bf16[32,24,2048]{2,1,0:T(8,128)(2,1)} %bitcast.176), calls=%async_computation.4 | async-start | bytes 6291456 | tf_op jit(solution)/shard_map/all_to_all | solution.py:94
  60.9 69.2 %all-gather.3.cloned.1.call-start = ((), (), s32[]{:S(2)}) async-start(), calls=%async_computation.6 | async-start | bytes 1572864 | tf_op jit(solution)/shard_map/all_gather | solution.py:31
  62.3 0.7 copy-start.2
  64.9 255.7 %all-gather.5.cloned.1.call-start = ((), (), s32[]{:S(2)}) async-start(), calls=%async_computation.7 | async-start | bytes 1769472 | tf_op jit(solution)/shard_map/all_gather | solution.py:104
  246.4 2.1 copy-start.1
  315.6 23.3 %copy-start.4 = (f32[384,2]{0,1:T(2,128)S(1)}, f32[384,2]{0,1:T(2,128)}, u32[]{:S(2)}) copy-start(f32[384,2]{0,1:T(2,128)} %param.9) | copy-start | bytes 9220
  315.6 13.3 %all-to-all-start.3 = ((bf16[4,2,1,128,256]{4,3,1,2,0:T(8,128)(2,1)}), bf16[4,2,1,128,256]{4,3,1,2,0:T(8,128)(2,1)S(1)}, u32[]{:S(2)}, u32[]{:S(2)}) async-start(bf16[4,2,1,128,256]{4,3,1,2,0:T(8,128)(2,1)} %copy.30), calls=%async_computation.3 | async-start | bytes 1048576 | tf_op jit(solution)/shard_map/all_to_all | solution.py:49
  328.9 33.4 %all-to-all-start.5 = ((bf16[32,24,256]{2,1,0:T(8,128)(2,1)}), bf16[32,24,256]{2,1,0:T(8,128)(2,1)S(1)}, u32[]{:S(2)}, u32[]{:S(2)}) async-start(bf16[32,24,256]{2,1,0:T(8,128)(2,1)} %bitcast.43), calls=%async_computation.5 | async-start | bytes 786432 | tf_op jit(solution)/shard_map/all_to_all | solution.py:115
Sparse Core Ops, SparseCore 0:
  65.0 65.1 all-gather.2
  250.3 28.7 all-gather.4
